TPU v7x, 512 devices: a whole 4x8x8 slice. The times are simulated.
512 devices in a mesh: row: 32 (over z, x), col: 16 (over y, core).
Axes of the slice: x: 4, y: 8, z: 8, core: 2. Of those that a mesh axis runs over, the one named last changes fastest.
Arguments:
- tokens: bfloat16 [32768, 2048], P('row'), may hold values from -136 to 136
- norm_gain: float32 [2048], replicated, may hold values from 0.1 to 1.9
- w_in: bfloat16 [2048, 1024], P(None, 'col'), may hold values from -0.125 to 0.125
- w_out: bfloat16 [1024, 2048], P(None, 'col'), may hold values from -0.1875 to 0.1875
Outputs:
- mixed_tokens: bfloat16 [32768, 2048], P('row', 'col')
All inputs are finite; a program needn't handle non-finite values.
Results may differ from a plain program's by a relative error of at most 0.013.
Values may be sent and summed in bfloat16 or wider, within the bound.
A program may use at most 64 MiB of HBM per device.

v0:
```python
import math

import jax
import jax.numpy as jnp
from jax import lax
from jax.sharding import PartitionSpec as P

GROUP = 256


NORM_EPS = 1e-06


def in_one_piece(arrays, axis, split_dim, concat_dim, along):
    ends, at = ([], 0)
    for a in arrays[:-1]:
        at += a.shape[along]
        ends.append(at)
    both = jnp.concatenate(arrays, axis=along)
    return tuple(
        jnp.split(
            lax.all_to_all(both, axis, split_axis=split_dim, concat_axis=concat_dim, tiled=True),
            ends,
            axis=along,
        )
    )


def as_sent(array):

    def short(part):
        return part.astype(jnp.bfloat16) if part.dtype == jnp.float32 else part

    return jax.tree.map(short, array)


def rotation_table(first_index, second_index, spectral_magnitude, factor):
    phase = (first_index * second_index % spectral_magnitude).astype(jnp.float32) * (
        2.0 * math.pi / spectral_magnitude
    )
    return (jnp.cos(phase) * factor, jnp.sin(phase) * factor)


def twiddle(real_input_values, imag_in, freq_index, pos_index, spectral_magnitude):
    cosine, sine = rotation_table(freq_index, pos_index, spectral_magnitude, 1.0)
    return (
        real_input_values * cosine + imag_in * sine,
        imag_in * cosine - real_input_values * sine,
    )


def second_section(stacked, half):
    length_dev = stacked.shape[1]
    stride = min(length_dev, 512)
    positions = lax.broadcasted_iota(jnp.int32, (length_dev, stride), 0)
    real_blocks = []
    imag_blocks = []
    for offset in range(0, length_dev, stride):
        freqs = lax.broadcasted_iota(jnp.int32, (length_dev, stride), 1) + offset
        cosine, sine = rotation_table(positions, freqs, length_dev, 1.0)
        with_cos = jnp.dot(stacked, cosine, precision=lax.Precision.HIGH)
        with_sin = jnp.dot(stacked, sine, precision=lax.Precision.HIGH)
        real_blocks.append(with_cos[:half] + with_sin[half:])
        imag_blocks.append(with_cos[half:] - with_sin[:half])
    return (jnp.concatenate(real_blocks, 1), jnp.concatenate(imag_blocks, 1))


def reorder_positions(arrived):
    channels, row_count, _, block_len = arrived.shape
    return jnp.swapaxes(arrived.reshape(channels, row_count, block_len), 1, 2).reshape(
        channels, row_count * block_len
    )


def local(tokens, norm_gain, w_in, w_out):
    length_dev = tokens.shape[0]
    row_count = lax.axis_size("row")
    col_count = lax.axis_size("col")
    total_len = length_dev * row_count
    widened = tokens.astype(jnp.float32)
    inverse = lax.rsqrt(jnp.mean(widened * widened, axis=1, keepdims=True) + NORM_EPS)
    normed = (widened * inverse * norm_gain[None, :]).astype(jnp.bfloat16)
    projected = lax.dot_general(
        w_in, normed, (((0,), (1,)), ((), ())), preferred_element_type=jnp.float32
    ).astype(jnp.bfloat16)
    channels = projected.shape[0]
    block_len = length_dev // row_count
    small_cos, small_sin = rotation_table(
        lax.broadcasted_iota(jnp.int32, (row_count, row_count), 0),
        lax.broadcasted_iota(jnp.int32, (row_count, row_count), 1),
        row_count,
        1.0 / math.sqrt(total_len),
    )
    per_row = channels // row_count
    arrived = lax.all_to_all(
        projected.reshape(channels, 1, length_dev), "row", split_axis=0, concat_axis=1, tiled=True
    )
    values = arrived.astype(jnp.float32)
    real_one = jnp.einsum("ka,cab->ckb", small_cos, values, precision=lax.Precision.HIGH)
    imag_one = -jnp.einsum("ka,cab->ckb", small_sin, values, precision=lax.Precision.HIGH)
    freq_index = lax.broadcasted_iota(jnp.int32, (row_count, length_dev), 0)
    pos_index = lax.broadcasted_iota(jnp.int32, (row_count, length_dev), 1)
    real_two, imag_two = twiddle(real_one, imag_one, freq_index, pos_index, total_len)
    stacked = jnp.concatenate(
        [
            real_two.reshape(per_row * row_count, length_dev),
            imag_two.reshape(per_row * row_count, length_dev),
        ],
        0,
    )
    real_three, imag_three = second_section(stacked, per_row * row_count)
    shaped = (per_row, row_count, row_count, block_len)
    back_real, back_imag = tuple(
        (
            part.astype(jnp.float32)
            for part in in_one_piece(
                (
                    real_three.reshape(shaped).astype(jnp.bfloat16),
                    imag_three.reshape(shaped).astype(jnp.bfloat16),
                ),
                "row",
                2,
                0,
                1,
            )
        )
    )
    spec_real = reorder_positions(back_real)
    spec_imag = reorder_positions(back_imag)
    quarter = length_dev // col_count
    group_cosine_table, group_sine_table = rotation_table(
        lax.broadcasted_iota(jnp.int32, (GROUP, GROUP), 0),
        lax.broadcasted_iota(jnp.int32, (GROUP, GROUP), 1),
        GROUP,
        1.0 / math.sqrt(GROUP),
    )
    real_input_values = lax.all_to_all(
        as_sent(spec_real.reshape(channels, col_count, quarter)),
        "col",
        split_axis=1,
        concat_axis=0,
        tiled=True,
    )
    imag_in = lax.all_to_all(
        as_sent(spec_imag.reshape(channels, col_count, quarter)),
        "col",
        split_axis=1,
        concat_axis=0,
        tiled=True,
    )
    width_all = real_input_values.shape[0]
    item_count = real_input_values.shape[2]
    groups = width_all // GROUP
    real_by_group = real_input_values.reshape(groups, GROUP, item_count)
    imaginary_by_group = imag_in.reshape(groups, GROUP, item_count)
    merged_spectrum = jnp.einsum(
        "hz,azo->aho", group_cosine_table, real_by_group, precision=lax.Precision.HIGH
    )
    merged_spectrum = merged_spectrum + jnp.einsum(
        "hz,azo->aho", group_sine_table, imaginary_by_group, precision=lax.Precision.HIGH
    )
    result = merged_spectrum.reshape(width_all, 1, item_count).astype(jnp.bfloat16)
    portion = lax.all_gather(result, "col", axis=2, tiled=True)
    flat = portion.reshape(portion.shape[0], portion.shape[2])
    output = lax.dot_general(
        flat, w_out, (((0,), (0,)), ((), ())), preferred_element_type=jnp.float32
    )
    return output.astype(jnp.bfloat16)


def solution(mesh):
    placed = (P("row", None), P(), P(None, "col"), P(None, "col"))
    return jax.shard_map(
        local, mesh=mesh, in_specs=placed, out_specs=P("row", "col"), check_vma=False
    )
```

profile of v0, /device:TPU:1, one launch (start us, length us, event | category | flops | bytes accessed | tf_op | source)
XLA Modules:
  0.0 170.5 jit_solution(13047247857492114618)
XLA Ops:
  6.5 3.2 %fusion = f32[1024]{0:T(1024)S(1)} fusion(bf16[1024,2048]{1,0:T(8,128)(2,1)} %param.4), kind=kLoop, calls=%fused_computation.2 | loop fusion | flops 6290432 | bytes 4198400 | tf_op jit(solution)/shard_map/reduce_sum | solution.py:81
  10.0 2.4 %fusion.38 = bf16[64,1,1024]{2,0,1:T(8,128)(2,1)S(1)} fusion(bf16[2048,64]{0,1:T(8,128)(2,1)} %param.6, bf16[1024,2048]{1,0:T(8,128)(2,1)S(1)} %copy-done.1, f32[2048]{0:T(1024)S(1)} %copy-done.2, f32[1024]{0:T(1024)S(1)} %add_rsqrt_fusion), kind=kOutput, calls=%fused_computation.44 | convolution fusion | flops 276889600 | bytes 4599808 | tf_op jit(solution)/shard_map/dot_general | solution.py:83
  13.0 0.7 reduce.1
  13.6 0.7 reshape.90
  14.3 13.9 %all-to-all-start = ((bf16[32,2,1024]{2,1,0:T(2,128)(2,1)}), bf16[32,2,1024]{2,1,0:T(2,128)(2,1)S(1)}, u32[]{:S(2)}, u32[]{:S(2)}) async-start(bf16[32,2,1024]{2,1,0:T(2,128)(2,1)} %reshape.90), calls=%async_computation | async-start | bytes 262144 | tf_op jit(solution)/shard_map/all_to_all | solution.py:95
  28.8 8.6 %all-to-all-done = bf16[32,2,1024]{2,1,0:T(2,128)(2,1)S(1)} async-done(((bf16[32,2,1024]{2,1,0:T(2,128)(2,1)}), bf16[32,2,1024]{2,1,0:T(2,128)(2,1)S(1)}, u32[]{:S(2)}, u32[]{:S(2)}) %all-to-all-start) | async-done | bytes 131104 | tf_op jit(solution)/shard_map/all_to_all | solution.py:95
  37.5 0.7 reduce
  38.9 8.7 %fusion.21 = f32[128,512]{1,0:T(8,128)S(1)} fusion(f32[64,1024]{1,0:T(8,128)S(1)} %bitcast.98, f32[64,1024]{1,0:T(8,128)S(1)} %bitcast.94), kind=kOutput, calls=%fused_computation.28 | convolution fusion | flops 410124288 | bytes 786432 | tf_op jit(solution)/shard_map/dot_general | solution.py:62
  47.6 8.6 %fusion.17 = f32[128,512]{1,0:T(8,128)S(1)} fusion(s32[512]{0:T(512)S(1)} %iota_add_fusion, f32[64,1024]{1,0:T(8,128)S(1)} %bitcast.99, f32[64,1024]{1,0:T(8,128)S(1)} %bitcast.95), kind=kOutput, calls=%fused_computation.24 | convolution fusion | flops 410124288 | bytes 788480 | tf_op jit(solution)/shard_map/dot_general | solution.py:61
  56.2 8.9 %fusion.15 = f32[128,512]{1,0:T(8,128)S(1)} fusion(s32[512]{0:T(512)S(1)} %iota_add_fusion, f32[64,1024]{1,0:T(8,128)S(1)} %bitcast.100, f32[64,1024]{1,0:T(8,128)S(1)} %bitcast.96), kind=kOutput, calls=%fused_computation.22 | convolution fusion | flops 410124288 | bytes 788480 | tf_op jit(solution)/shard_map/dot_general | solution.py:62
  65.1 8.6 %fusion.23 = f32[128,512]{1,0:T(8,128)S(1)} fusion(f32[64,1024]{1,0:T(8,128)S(1)} %bitcast.101, f32[64,1024]{1,0:T(8,128)S(1)} %bitcast.97), kind=kOutput, calls=%fused_computation.30 | convolution fusion | flops 410124288 | bytes 786432 | tf_op jit(solution)/shard_map/dot_general | solution.py:61
  74.2 0.7 copy.35
  76.6 13.7 %all_to_all.66 = bf16[32,2,2048]{2,1,0:T(2,128)(2,1)S(1)} all-to-all(bf16[32,2,2048]{2,1,0:T(2,128)(2,1)S(1)} %reshape.92), channel_id=1, replica_groups=mesh['row'=32,'col'=16] {'row'}, dimensions={0} | all-to-all | bytes 524288 | tf_op jit(solution)/shard_map/all_to_all | solution.py:22
  91.5 0.9 reshape.96
  92.4 10.9 %all-to-all-start.3 = ((bf16[16,2,2048]{2,1,0:T(2,128)(2,1)}), bf16[16,2,2048]{2,1,0:T(2,128)(2,1)S(1)}, u32[]{:S(2)}, u32[]{:S(2)}) async-start(bf16[16,2,2048]{2,1,0:T(2,128)(2,1)} %reshape.96), calls=%async_computation.3 | async-start | bytes 262144 | tf_op jit(solution)/shard_map/all_to_all | solution.py:144
  103.9 0.9 reshape.94
  104.8 7.4 %all-to-all-done.3 = bf16[16,2,2048]{2,1,0:T(2,128)(2,1)S(1)} async-done(((bf16[16,2,2048]{2,1,0:T(2,128)(2,1)}), bf16[16,2,2048]{2,1,0:T(2,128)(2,1)S(1)}, u32[]{:S(2)}, u32[]{:S(2)}) %all-to-all-start.3) | async-done | bytes 131104 | tf_op jit(solution)/shard_map/all_to_all | solution.py:144
  112.2 3.4 %all-to-all-start.2 = ((bf16[16,2,2048]{2,1,0:T(2,128)(2,1)}), bf16[16,2,2048]{2,1,0:T(2,128)(2,1)S(1)}, u32[]{:S(2)}, u32[]{:S(2)}) async-start(bf16[16,2,2048]{2,1,0:T(2,128)(2,1)} %reshape.94), calls=%async_computation.2 | async-start | bytes 262144 | tf_op jit(solution)/shard_map/all_to_all | solution.py:137
  116.3 8.2 %all-to-all-done.2 = bf16[16,2,2048]{2,1,0:T(2,128)(2,1)S(1)} async-done(((bf16[16,2,2048]{2,1,0:T(2,128)(2,1)}), bf16[16,2,2048]{2,1,0:T(2,128)(2,1)S(1)}, u32[]{:S(2)}, u32[]{:S(2)}) %all-to-all-start.2) | async-done | bytes 131104 | tf_op jit(solution)/shard_map/all_to_all | solution.py:137
  125.2 1.2 fusion.49
  126.4 1.2 fusion.37
  127.7 0.7 convert_element_type.118
  128.5 32.2 %all-gather.2.cloned.1.call-done = bf16[1024,1,1024]{0,2,1:T(8,128)(2,1)} async-done(((bf16[1024,1,64]{0,2,1:T(8,128)(2,1)}), bf16[1024,1,1024]{0,2,1:T(8,128)(2,1)}) %all-gather.2.cloned.1.call-update) | async-done | bytes 2097168 | tf_op jit(solution)/shard_map/all_gather | solution.py:163
  160.7 3.0 %fusion.29 = bf16[1024,128]{1,0:T(8,128)(2,1)} fusion(bf16[1024,128]{1,0:T(8,128)(2,1)S(1)} %copy-done, bf16[1024,1,1024]{0,2,1:T(8,128)(2,1)} %all-gather.2.cloned.1.call-done), kind=kOutput, calls=%fused_computation.36 | convolution fusion | flops 268566528 | bytes 2621440 | tf_op jit(solution)/shard_map/dot_general | solution.py:165
  (40 shorter events, 7.4 us)
Async XLA Ops:
  6.5 154.2 %copy-start = (bf16[1024,128]{1,0:T(8,128)(2,1)S(1)}, bf16[1024,128]{1,0:T(8,128)(2,1)}, u32[]{:S(2)}) copy-start(bf16[1024,128]{1,0:T(8,128)(2,1)} %param.7) | copy-start | bytes 786436
  6.5 3.5 %copy-start.1 = (bf16[1024,2048]{1,0:T(8,128)(2,1)S(1)}, bf16[1024,2048]{1,0:T(8,128)(2,1)}, u32[]{:S(2)}) copy-start(bf16[1024,2048]{1,0:T(8,128)(2,1)} %param.4) | copy-start | bytes 12582916
  6.5 3.5 %copy-start.2 = (f32[2048]{0:T(1024)S(1)}, f32[2048]{0:T(1024)}, u32[]{:S(2)}) copy-start(f32[2048]{0:T(1024)} %param.5) | copy-start | bytes 24580
  14.3 23.1 %all-to-all-start = ((bf16[32,2,1024]{2,1,0:T(2,128)(2,1)}), bf16[32,2,1024]{2,1,0:T(2,128)(2,1)S(1)}, u32[]{:S(2)}, u32[]{:S(2)}) async-start(bf16[32,2,1024]{2,1,0:T(2,128)(2,1)} %reshape.90), calls=%async_computation | async-start | bytes 262144 | tf_op jit(solution)/shard_map/all_to_all | solution.py:95
  92.4 19.8 %all-to-all-start.3 = ((bf16[16,2,2048]{2,1,0:T(2,128)(2,1)}), bf16[16,2,2048]{2,1,0:T(2,128)(2,1)S(1)}, u32[]{:S(2)}, u32[]{:S(2)}) async-start(bf16[16,2,2048]{2,1,0:T(2,128)(2,1)} %reshape.96), calls=%async_computation.3 | async-start | bytes 262144 | tf_op jit(solution)/shard_map/all_to_all | solution.py:144
  112.2 12.3 %all-to-all-start.2 = ((bf16[16,2,2048]{2,1,0:T(2,128)(2,1)}), bf16[16,2,2048]{2,1,0:T(2,128)(2,1)S(1)}, u32[]{:S(2)}, u32[]{:S(2)}) async-start(bf16[16,2,2048]{2,1,0:T(2,128)(2,1)} %reshape.94), calls=%async_computation.2 | async-start | bytes 262144 | tf_op jit(solution)/shard_map/all_to_all | solution.py:137
  115.6 45.1 %all-gather.2.cloned.1.call-start = ((), (), s32[]{:S(2)}) async-start(), calls=%async_computation.4 | async-start | bytes 2228224 | tf_op jit(solution)/shard_map/all_gather | solution.py:163
Sparse Core Ops, SparseCore 0:
  128.6 32.0 all-gather.1
where the time goes:
time: 171 us
  waiting for transfers between devices  56.5 us (33%)
  matrix products  43.2 us (25%)
  starting transfers between devices  28.2 us (16%)
  blocking collectives  13.7 us (8%)
  between operations  13.7 us (8%)
  local copies, waits for them, and re-layouts  9.71 us (6%)
  other arithmetic  5.56 us (3%)
    all_gather x1, waiting for transfers between devices, local(): portion = lax.all_gather(result, 'col', axis=2, tiled=True)  32.2 us
    dot_general x2, matrix products, second_section(): with_sin = jnp.dot(stacked, sine, precision=lax.Precision.HIGH)  17.6 us
    dot_general x2, matrix products, second_section(): with_cos = jnp.dot(stacked, cosine, precision=lax.Precision.HIGH)  17.2 us
    all_to_all x1, starting transfers between devices, local(): lax.all_to_all(projected.reshape(channels, 1, length_dev), 'row', split_a...  13.9 us
    all_to_all x1, blocking collectives, in_one_piece(): lax.all_to_all(both, axis, split_axis=split_dim, concat_axis=concat_dim,...  13.7 us
    all_to_all x1, starting transfers between devices, local(): lax.all_to_all(as_sent(spec_imag.reshape(channels, col_count, quarter)),...  10.9 us
    all_to_all x1, waiting for transfers between devices, local(): lax.all_to_all(projected.reshape(channels, 1, length_dev), 'row', split_a...  8.62 us
    all_to_all x1, waiting for transfers between devices, local(): lax.all_to_all(as_sent(spec_real.reshape(channels, col_count, quarter)),...  8.24 us
  transfers between devices with their start and end apart: 4, of which 4 were waited for; matrix products, arithmetic and copies ran while one was open for 2% of the time, Pallas kernels for 0%

commit v1 on v0

v1 whole, which is shorter than its diff:
```python
import functools
import math

import jax
import jax.numpy as jnp
import ml_dtypes
import numpy as np
from jax import lax
from jax.experimental import pallas as pl
from jax.experimental.pallas import tpu as pltpu
from jax.sharding import PartitionSpec as P

GROUP = 256
NORM_EPS = 1e-06
LANES = 128
PIECES = 4
MESH = pl.DeviceIdType.MESH
BF16 = jnp.bfloat16
F32 = jnp.float32


def angle(first, second, period):
    return (np.multiply.outer(first, second) % period) * (2.0 * math.pi / period)


def tables(rows, width, length):
    subs = GROUP // width
    pairs = np.arange(GROUP // 2)
    channel = np.arange(GROUP)
    cosine, sine = np.cos(angle(pairs, channel, GROUP)), np.sin(angle(pairs, channel, GROUP))
    sine[0] = np.cos(math.pi * channel)
    mix = np.stack([cosine, sine], 1).reshape(GROUP, GROUP) / math.sqrt(GROUP)

    back = np.zeros((subs, 2, rows, GROUP))
    for p in range(GROUP // 2):
        j, r = divmod(p, rows)
        if p == 0:
            back[j, 0, r, 0] = 1.0
            back[j, 1, r, GROUP // 2] = 1.0
        else:
            back[j, 0, r, p] = back[j, 0, r, GROUP - p] = 1.0
            back[j, 1, r, GROUP - p] = 1.0
            back[j, 1, r, p] = -1.0
    back = back.reshape(GROUP, GROUP)

    total = rows * length
    high = total // LANES
    steps = length // LANES
    a = np.arange(high)
    turn = angle(a, a, high)
    outer = np.zeros((2, 2, high, rows, 2, steps))
    for s in range(2):
        outer[s, 0, :, :, s, :] = np.cos(turn).reshape(high, rows, steps)
        outer[s, 1, :, :, s, :] = -np.sin(turn).reshape(high, rows, steps)
    outer = outer.reshape(4 * high, 2 * high) / math.sqrt(high)

    b = np.arange(LANES)
    twist = angle(a, b, total)
    twist = np.concatenate([np.cos(twist), np.sin(twist)], 0)

    turn = angle(b, b, LANES)
    cosine, sine = np.cos(turn), np.sin(turn)
    inner = np.stack([np.concatenate([cosine, sine], 1), np.concatenate([sine, -cosine], 1)]) / math.sqrt(LANES)
    short = ml_dtypes.bfloat16
    return mix.astype(short), back.astype(short), outer.astype(short), twist.astype(np.float32), inner.astype(short), np.eye(width).astype(short)


def nt(a, b):
    return lax.dot_general(a, b, (((1,), (1,)), ((), ())), preferred_element_type=F32)


def nn(a, b):
    return jnp.dot(a, b, preferred_element_type=F32)


def kernel(
    rows, cols,
    tokens, gain, w_in, w_out, mix, back, outer, twist, inner, eye, out,
    tok_v, tg_v, sq_v, gain_v, win_v, wout_v, mix_v, back_v, outer_v, twist_v, inner_v, eye_v,
    x_v, wide_v, a_v, ar_v, b_v, br_v, s_v, wt_v, acc_v,
    tok_sem, tab_sem, xs_sem, xr_sem, as_sem, ar_sem, bs_sem, br_sem, gs_sem, gr_sem, cs_sem, cr_sem,
):
    length, features = tokens.shape
    width = w_in.shape[1]
    subs = GROUP // width
    piece = length // PIECES
    steps = length // LANES
    tile = 2 * steps
    row, col = lax.axis_index("row"), lax.axis_index("col")
    core = lax.rem(col, 2)
    other = col + 1 - 2 * core
    chip = lax.div(col, 2)
    twin = col + 2 - 4 * lax.rem(chip, 2)
    right, left = lax.rem(col + 2, cols), lax.rem(col + cols - 2, cols)
    j = lax.rem(col, subs)

    def load(src, dst, sem):
        return pltpu.make_async_copy(src, dst, sem)

    def send(src, dst, send_sem, recv_sem, device):
        return pltpu.make_async_remote_copy(
            src_ref=src, dst_ref=dst, send_sem=send_sem, recv_sem=recv_sem, device_id=device, device_id_type=MESH
        )

    loads = [load(gain, gain_v, tab_sem.at[0]), load(w_in, win_v, tab_sem.at[1]), load(eye, eye_v, tab_sem.at[2])]
    for c in loads:
        c.start()
    tok = [
        load(tokens.at[pl.ds(p * piece, piece)], tok_v.at[pl.ds(p * piece, piece)], tok_sem.at[p]) for p in range(PIECES)
    ]
    for c in tok:
        c.start()
    later = [
        load(src, dst, tab_sem.at[3 + i])
        for i, (src, dst) in enumerate(
            ((mix, mix_v), (outer, outer_v), (w_out, wout_v), (back, back_v), (twist, twist_v), (inner, inner_v))
        )
    ]
    for c in later:
        c.start()

    barrier = pltpu.get_barrier_semaphore()
    for mate in (other, right, left):
        pl.semaphore_signal(barrier, inc=1, device_id=(row, mate), device_id_type=MESH)

    def greet(i, carry):
        pl.semaphore_signal(barrier, inc=1, device_id=(lax.rem(row + i, rows), col), device_id_type=MESH)
        return carry

    lax.fori_loop(1, rows, greet, 0)

    for c in loads:
        c.wait()

    def x_slot(p, who):
        return x_v.at[p, pl.ds(pl.multiple_of(lax.rem(who, subs) * width, width), width)]

    to_other = [send(x_slot(p, col), x_slot(p, col), xs_sem.at[0, p], xr_sem.at[0, p], (row, other)) for p in range(PIECES)]
    to_twin = [send(x_slot(p, col), x_slot(p, col), xs_sem.at[1, p], xr_sem.at[1, p], (row, twin)) for p in range(PIECES)]
    onward = [send(x_slot(p, twin), x_slot(p, twin), xs_sem.at[2, p], xr_sem.at[2, p], (row, other)) for p in range(PIECES)]
    block = 64
    for p in range(PIECES):
        tok[p].wait()

        def scaled(i, carry):
            at = pl.multiple_of(i * block, block)
            t = tok_v[pl.ds(p * piece + at, block), :].astype(F32)
            sq_v[pl.ds(at, block), :] = jnp.broadcast_to(jnp.sum(t * t, axis=1, keepdims=True), (block, LANES))
            tg_v[pl.ds(at, block), :] = (t * gain_v[...]).astype(BF16)
            return carry

        lax.fori_loop(0, piece // block, scaled, 0)
        x = nn(tg_v[...], win_v[...])
        x = x * lax.rsqrt(sq_v[:, :width] * (1.0 / features) + NORM_EPS)
        x_v[p, pl.ds(pl.multiple_of(j * width, width), width), :] = nt(eye_v[...], x.astype(BF16)).astype(BF16)
        if p == 0:
            pl.semaphore_wait(barrier, rows + 2)
        to_twin[p].start()
        to_other[p].start()
    for p in range(PIECES):
        to_twin[p].wait_recv()
        onward[p].start()

    for c in later:
        c.wait()
    mine = mix_v[pl.ds(pl.multiple_of(j * width, width), width), :]
    for p in range(PIECES):
        to_other[p].wait_recv()
        onward[p].wait_recv()
        y = nn(mine, x_v[p])
        for t in range(piece // LANES):
            wide_v[pl.ds(p * (piece // LANES) + t, width, stride=steps), :] = y[:, t * LANES : (t + 1) * LANES]
    a_v[...] = wide_v[...].astype(BF16)

    def spread(src_v, dst_v, send_sem, recv_sem):
        own = pl.ds(pl.multiple_of(row * tile, tile), tile)

        def one(i, carry):
            d = lax.rem(row + i, rows)
            send(
                src_v.at[pl.ds(pl.multiple_of(d * tile, tile), tile)], dst_v.at[own], send_sem, recv_sem, (d, col)
            ).start()
            return carry

        lax.fori_loop(1, rows, one, 0)
        dst_v[own, :] = src_v[own, :]

    rest = pl.ds(0, (rows - 1) * tile)
    spread(a_v, ar_v, as_sem, ar_sem)

    per_group = 2 * LANES // GROUP if GROUP < 2 * LANES else GROUP // (2 * width)
    for g in range(cols // subs):
        wp = nn(back_v[...], wout_v[pl.ds(g * GROUP, GROUP), :])
        for i in range(per_group):
            wt_v[g * per_group + i] = jnp.transpose(wp[i * 2 * width : (i + 1) * 2 * width]).astype(BF16)

    load(ar_v.at[rest], ar_v.at[rest], ar_sem).wait()

    first = nn(outer_v[...], ar_v[...])
    high = rows * steps
    twist_cos, twist_sin = twist_v[:high], twist_v[high:]
    special = lax.min(j * rows + row, 1)
    for s in range(2):
        re = first[2 * s * high : (2 * s + 1) * high]
        im = first[(2 * s + 1) * high : (2 * s + 2) * high]
        turned = jnp.concatenate([re * twist_cos + im * twist_sin, im * twist_cos - re * twist_sin], axis=1).astype(BF16)
        u = nt(inner_v[0] if s == 0 else inner_v[special], turned)
        for t in range(2):
            wide_v[pl.ds(2 * t + s, LANES, stride=4), :] = u[:, t * LANES : (t + 1) * LANES]
    b_v[...] = wide_v[...].astype(BF16)

    spread(b_v, br_v, bs_sem, br_sem)
    load(br_v.at[rest], br_v.at[rest], br_sem).wait()
    wide_v[...] = br_v[...].astype(F32)
    for q in range(steps):
        for s in range(2):
            s_v[col, s * rows : (s + 1) * rows, q * LANES : (q + 1) * LANES] = wide_v[
                pl.ds(2 * q + s, rows, stride=tile), :
            ].astype(BF16)

    chips = cols // 2
    half = chips // 2
    part = width // PIECES

    def slot(who, q):
        return s_v.at[who, pl.ds(q * part, part)]

    def ring(d, t, q):
        who = lax.rem(col + (cols - 2 * (t - 1) if d == 0 else 2 * (t - 1)), cols)
        return send(slot(who, q), slot(who, q), gs_sem.at[d, t - 1, q], gr_sem.at[d, t - 1, q], (row, right if d == 0 else left))

    def relay(d, t, q):
        who = lax.rem(col + (cols - 2 * t if d == 0 else 2 * t), cols)
        return send(slot(who, q), slot(who, q), cs_sem.at[d, t, q], cr_sem.at[d, t, q], (row, other))

    def uses(d, t):
        if t < half:
            return range(PIECES)
        return range(PIECES // 2) if d == 0 else range(PIECES // 2, PIECES)

    sent = []
    for q in range(PIECES):
        for d in range(2):
            sent.append(ring(d, 1, q))
            sent[-1].start()
    for q in range(PIECES):
        sent.append(relay(0, 0, q))
        sent[-1].start()

    def add(which):
        s = s_v[pl.ds(2 * which, 2)].reshape(2 * width, length)
        acc_v[...] += nn(wt_v[which], s)

    acc_v[...] = jnp.zeros_like(acc_v)
    for q in range(PIECES):
        relay(0, 0, q).wait_recv()
    add(chip)
    for t in range(1, half + 1):
        for q in range(PIECES):
            for d in range(2):
                if q in uses(d, t):
                    ring(d, t, q).wait_recv()
                    if t < half and q in uses(d, t + 1):
                        sent.append(ring(d, t + 1, q))
                        sent[-1].start()
                    sent.append(relay(d, t, q))
                    sent[-1].start()
        for d in range(2):
            for q in uses(d, t):
                relay(d, t, q).wait_recv()
        if t < half:
            add(lax.rem(chip + chips - t, chips))
        add(lax.rem(chip + t, chips))
    for i in range(length // LANES):
        out[i * LANES : (i + 1) * LANES, :] = jnp.transpose(acc_v[:, i * LANES : (i + 1) * LANES]).astype(BF16)

    for c in to_other + to_twin + onward + sent:
        c.wait_send()
    load(a_v.at[rest], a_v.at[rest], as_sem).wait()
    load(b_v.at[rest], b_v.at[rest], bs_sem).wait()


def local(rows, cols, tokens, norm_gain, w_in, w_out):
    length, features = tokens.shape
    width, mapped = w_in.shape[1], w_out.shape[1]
    mix, back, outer, twist, inner, eye = tables(rows, width, length)
    high = rows * length // LANES
    half = cols // 4
    any_spec = pl.BlockSpec(memory_space=pl.ANY)
    dma = pltpu.SemaphoreType.DMA
    return pl.pallas_call(
        functools.partial(kernel, rows, cols),
        out_shape=jax.ShapeDtypeStruct((length, mapped), BF16),
        in_specs=[any_spec] * 10,
        out_specs=pl.BlockSpec(memory_space=pltpu.VMEM),
        scratch_shapes=[
            pltpu.VMEM((length, features), BF16),
            pltpu.VMEM((length // PIECES, features), BF16),
            pltpu.VMEM((length // PIECES, LANES), F32),
            pltpu.VMEM((1, features), F32),
            pltpu.VMEM((features, width), BF16),
            pltpu.VMEM(w_out.shape, BF16),
            pltpu.VMEM(mix.shape, BF16),
            pltpu.VMEM(back.shape, BF16),
            pltpu.VMEM(outer.shape, BF16),
            pltpu.VMEM(twist.shape, F32),
            pltpu.VMEM(inner.shape, BF16),
            pltpu.VMEM(eye.shape, BF16),
            pltpu.VMEM((PIECES, GROUP, length // PIECES), BF16),
            pltpu.VMEM((2 * high, LANES), F32),
            pltpu.VMEM((2 * high, LANES), BF16),
            pltpu.VMEM((2 * high, LANES), BF16),
            pltpu.VMEM((2 * high, LANES), BF16),
            pltpu.VMEM((2 * high, LANES), BF16),
            pltpu.VMEM((cols, width, length), BF16),
            pltpu.VMEM((cols // 2, mapped, 2 * width), BF16),
            pltpu.VMEM((mapped, length), F32),
            dma((PIECES,)),
            dma((9,)),
            dma((3, PIECES)),
            dma((3, PIECES)),
            dma,
            dma,
            dma,
            dma,
            dma((2, half, PIECES)),
            dma((2, half, PIECES)),
            dma((2, half + 1, PIECES)),
            dma((2, half + 1, PIECES)),
        ],
        compiler_params=pltpu.CompilerParams(
            collective_id=0, has_side_effects=True, vmem_limit_bytes=60 * 1024 * 1024
        ),
    )(tokens, norm_gain.reshape(1, features), w_in, w_out, mix, back, outer, twist, inner, eye)


def solution(mesh):
    placed = (P("row", None), P(), P(None, "col"), P(None, "col"))
    return jax.shard_map(
        functools.partial(local, mesh.shape["row"], mesh.shape["col"]),
        mesh=mesh,
        in_specs=placed,
        out_specs=P("row", "col"),
        check_vma=False,
    )
```

time: 171 us -> 61.8 us (0.36)
  Pallas kernels: 0 us -> 58 us
  waiting for transfers between devices: 56.5 us -> 0 us
  matrix products: 43.2 us -> 0 us
  starting transfers between devices: 28.2 us -> 0 us
  blocking collectives: 13.7 us -> 0 us
  between operations: 13.7 us -> 0.01 us
  local copies, waits for them, and re-layouts: 9.71 us -> 3.62 us
  other arithmetic: 5.56 us -> 0 us
    pallas_call x0 -> x1, Pallas kernels: none -> 58 us  [local(): pl.pallas_call(functools.partial(kernel, rows, cols), out_shape=jax.Shape...]
    dot_general x10 -> x0, matrix products: 43.2 us -> none  [the longest x2 17.6 us: second_section(): with_sin = jnp.dot(stacked, sine, precision=lax.Precision.HIGH)]
    all_gather x1 -> x0, waiting for transfers between devices: 32.2 us -> none  [local(): portion = lax.all_gather(result, 'col', axis=2, tiled=True)]
    all_to_all x3 -> x0, starting transfers between devices: 28.2 us -> none  [the longest x1 13.9 us: local(): lax.all_to_all(projected.reshape(channels, 1, length_dev), 'row', split_a...]
    all_to_all x3 -> x0, waiting for transfers between devices: 24.2 us -> none  [the longest x1 8.62 us: local(): lax.all_to_all(projected.reshape(channels, 1, length_dev), 'row', split_a...]
    all_to_all x1 -> x0, blocking collectives: 13.7 us -> none  [in_one_piece(): lax.all_to_all(both, axis, split_axis=split_dim, concat_axis=concat_dim,...]
    convert_element_type x9 -> x0, local copies, waits for them, and re-layouts: 4.28 us -> none  [the longest x3 1.39 us: short(): return part.astype(jnp.bfloat16) if part.dtype == jnp.float32 else part]
    reduce_sum x1 -> x0, other arithmetic: 3.22 us -> none  [local(): jnp.mean(widened * widened, axis=1, keepdims=True) + NORM_EPS]
  transfers between devices with their start and end apart: 4 -> 0, of which waited for: 4 -> 0; matrix products, arithmetic and copies ran while one was open for 2% -> 0% of each run, Pallas kernels for 0% -> 0%
where the time goes in v1:
time: 61.8 us; the launch traced here: 61.7 us
  Pallas kernels  58 us (94%)
  local copies, waits for them, and re-layouts  3.62 us (6%)
    pallas_call x1, Pallas kernels, local(): pl.pallas_call(functools.partial(kernel, rows, cols), out_shape=jax.Shape...  58 us
    unnamed x2, local copies, waits for them, and re-layouts  3.62 us

profile of v1, /device:TPU:1, one launch (start us, length us, event | category | flops | bytes accessed | tf_op | source)
XLA Modules:
  0.0 61.7 jit_solution(12731584866651340882)
XLA Ops:
  0.0 1.9 %copy.11.w_in = bf16[2048,64]{1,0:T(8,128)(2,1)} copy(bf16[2048,64]{0,1:T(8,128)(2,1)} %param.12) | data formatting | bytes 524288 | tf_op args[2]
  1.9 58.0 %shard_map.100 = bf16[1024,128]{1,0:T(8,128)(2,1)} custom-call(bf16[1024,2048]{1,0:T(8,128)(2,1)} %tokens.1, f32[1,2048]{1,0:T(1,128)} %bitcast.1, bf16[2048,64]{1,0:T(8,128)(2,1)} %copy.11.w_in, bf16[1024,128]{1,0:T(8,128)(2,1)} %w_out.1, bf16[256,256]{1,0:T(8,128)(2,1)} %constant.12.clone.mix, bf16[256,256]{1,0:T(8,128)(2,1)} %constant.13.clone.back, ...), custom_call_target="tpu_custom_call" | custom-call | tf_op jit(solution)/shard_map/pallas_call | solution.py:291
  60.0 1.7 %copy.13 = bf16[1024,128]{1,0:T(8,128)(2,1)} copy(bf16[1024,128]{1,0:T(8,128)(2,1)} %shard_map.100) | data formatting | bytes 524288

commit v2 on v1

v2 whole, which is shorter than its diff:
```python
import functools
import math

import jax
import jax.numpy as jnp
import ml_dtypes
import numpy as np
from jax import lax
from jax.experimental import pallas as pl
from jax.experimental.pallas import tpu as pltpu
from jax.sharding import PartitionSpec as P

GROUP = 256
NORM_EPS = 1e-06
LANES = 128
X_SIDE = 4
Z_SIDE = 8
PIECES = 4
HALVES = 2
SETS = 4
MESH = pl.DeviceIdType.MESH
FARTHEST_FIRST = sorted(
    [(dz, dx) for dz in range(Z_SIDE) for dx in range(X_SIDE) if dz or dx],
    key=lambda o: (-min(o[0], Z_SIDE - o[0]) - min(o[1], X_SIDE - o[1]), o),
)
BF16 = jnp.bfloat16
F32 = jnp.float32

NEAREST_FIRST = FARTHEST_FIRST[::-1]


def angle(first, second, period):
    return (np.multiply.outer(first, second) % period) * (2.0 * math.pi / period)


def tables(rows, width, length):
    subs = GROUP // width
    pairs = np.arange(GROUP // 2)
    channel = np.arange(GROUP)
    cosine, sine = np.cos(angle(pairs, channel, GROUP)), np.sin(angle(pairs, channel, GROUP))
    sine[0] = np.cos(math.pi * channel)
    mix = np.stack([cosine, sine], 1).reshape(GROUP, GROUP) / math.sqrt(GROUP)

    back = np.zeros((subs, 2, rows, GROUP))
    for p in range(GROUP // 2):
        j, r = divmod(p, rows)
        if p == 0:
            back[j, 0, r, 0] = 1.0
            back[j, 1, r, GROUP // 2] = 1.0
        else:
            back[j, 0, r, p] = back[j, 0, r, GROUP - p] = 1.0
            back[j, 1, r, GROUP - p] = 1.0
            back[j, 1, r, p] = -1.0
    back = back.reshape(subs, 2, SETS, rows // SETS, GROUP).transpose(0, 2, 1, 3, 4).reshape(GROUP, GROUP)

    total = rows * length
    high = total // LANES
    steps = length // LANES
    a = np.arange(high)
    turn = angle(a, a, high)
    outer = np.zeros((2, 2, high, rows, 2, steps))
    for s in range(2):
        outer[s, 0, :, :, s, :] = np.cos(turn).reshape(high, rows, steps)
        outer[s, 1, :, :, s, :] = -np.sin(turn).reshape(high, rows, steps)
    outer = outer.reshape(4 * high, 2 * high) / math.sqrt(high)

    b = np.arange(LANES)
    twist = angle(a, b, total)
    twist = np.concatenate([np.cos(twist), np.sin(twist)], 0)

    turn = angle(b, b, LANES)
    cosine, sine = np.cos(turn), np.sin(turn)
    inner = np.stack([np.concatenate([cosine, sine], 1), np.concatenate([sine, -cosine], 1)]) / math.sqrt(LANES)
    short = ml_dtypes.bfloat16
    return mix.astype(short), back.astype(short), outer.astype(short), twist.astype(np.float32), inner.astype(short), np.eye(width).astype(short)


def nt(a, b):
    return lax.dot_general(a, b, (((1,), (1,)), ((), ())), preferred_element_type=F32)


def nn(a, b):
    return jnp.dot(a, b, preferred_element_type=F32)


def kernel(
    rows, cols,
    tokens, gain, w_in, w_out, mix, back, outer, twist, inner, eye, out,
    tok_v, wg_v, gain_v, win_v, wout_v, mix_v, back_v, outer_v, twist_v, inner_v, eye_v,
    x_v, wide_v, a_v, ar_v, b_v, br_v, s_v, wt_v, acc_v, out_v,
    tok_sem, tab_sem, near_sem, xs_sem, xr_sem, as_sem, ar_sem, bs_sem, br_sem, gs_sem, gr_sem, cs_sem, cr_sem,
):
    length, features = tokens.shape
    width = w_in.shape[0]
    subs = GROUP // width
    piece = length // PIECES
    steps = length // LANES
    tile = 2 * steps
    row, col = lax.axis_index("row"), lax.axis_index("col")
    core = lax.rem(col, 2)
    other = col + 1 - 2 * core
    chip = lax.div(col, 2)
    twin = col + 2 - 4 * lax.rem(chip, 2)
    right, left = lax.rem(col + 2, cols), lax.rem(col + cols - 2, cols)
    j = lax.rem(col, subs)

    def load(src, dst, sem):
        return pltpu.make_async_copy(src, dst, sem)

    def send(src, dst, send_sem, recv_sem, device):
        return pltpu.make_async_remote_copy(
            src_ref=src, dst_ref=dst, send_sem=send_sem, recv_sem=recv_sem, device_id=device, device_id_type=MESH
        )

    z, x = lax.div(row, X_SIDE), lax.rem(row, X_SIDE)
    beside = [(lax.rem(z + Z_SIDE + o, Z_SIDE) * X_SIDE + x, col) for o in (1, -1, 2, -2)]
    near = beside + [(row, other), (row, right), (row, left)]
    near += [(z * X_SIDE + lax.rem(x + i, X_SIDE), col) for i in range(1, X_SIDE)]
    barrier = pltpu.get_barrier_semaphore()
    for mate in near:
        pl.semaphore_signal(barrier, inc=1, device_id=mate, device_id_type=MESH)

    def tell(i):
        for k, mate in enumerate(beside):
            pl.semaphore_signal(near_sem.at[i, k], inc=1, device_id=mate, device_id_type=MESH)

    def hear(i):
        for k in range(len(beside)):
            pl.semaphore_wait(near_sem.at[i, k], 1)

    loads = [load(gain, gain_v, tab_sem.at[0]), load(w_in, win_v, tab_sem.at[1]), load(eye, eye_v, tab_sem.at[2])]
    for c in loads:
        c.start()
    tok = [
        load(tokens.at[pl.ds(p * piece, piece)], tok_v.at[pl.ds(p * piece, piece)], tok_sem.at[p]) for p in range(PIECES)
    ]
    for c in tok:
        c.start()
    later = [
        load(src, dst, tab_sem.at[3 + i])
        for i, (src, dst) in enumerate(
            ((mix, mix_v), (outer, outer_v), (w_out, wout_v), (back, back_v), (twist, twist_v), (inner, inner_v))
        )
    ]
    for c in later:
        c.start()
    with jax.named_scope("wload"):
        for c in loads:
            c.wait()
        wg_v[...] = (win_v[...].astype(F32) * gain_v[...]).astype(BF16)

    def x_slot(p, who):
        return x_v.at[p, pl.ds(pl.multiple_of(lax.rem(who, subs) * width, width), width)]

    to_other = [send(x_slot(p, col), x_slot(p, col), xs_sem, xr_sem.at[0, p], (row, other)) for p in range(PIECES)]
    to_twin = [send(x_slot(p, col), x_slot(p, col), xs_sem, xr_sem.at[1, p], (row, twin)) for p in range(PIECES)]
    onward = [send(x_slot(p, twin), x_slot(p, twin), xs_sem, xr_sem.at[0, p], (row, other)) for p in range(PIECES)]
    block = 64
    for p in range(PIECES):
        with jax.named_scope(f"tokwait{p}"):
            tok[p].wait()
        with jax.named_scope(f"proj{p}"):
            y = nt(tok_v[p * piece : (p + 1) * piece, :], wg_v[...])
            squares = []
            for b in range(piece // block):
                total = jnp.zeros((block, LANES), F32)
                for f in range(0, features, LANES):
                    t = tok_v[pl.ds(p * piece + b * block, block), f : f + LANES].astype(F32)
                    total = total + t * t
                squares.append(jnp.sum(total, axis=1, keepdims=True))
            y = y * lax.rsqrt(jnp.concatenate(squares, 0) * (1.0 / features) + NORM_EPS)
            x_v[p, pl.ds(pl.multiple_of(j * width, width), width), :] = nt(eye_v[...], y.astype(BF16)).astype(BF16)
        if p == 0:
            with jax.named_scope("near"):
                pl.semaphore_wait(barrier, len(near))
            tell(0)
        to_twin[p].start()
        to_other[p].start()
    with jax.named_scope("hear0"):
        hear(0)
        tell(1)

    for c in later:
        c.wait()
    mine = mix_v[pl.ds(pl.multiple_of(j * width, width), width), :]
    for p in range(PIECES + 1):
        if p < PIECES:
            with jax.named_scope(f"twin{p}"):
                to_twin[p].wait_recv()
                onward[p].start()
        if p > 0:
            with jax.named_scope(f"group{p - 1}"):
                both = x_v.at[p - 1, pl.ds(0, 2 * width)]
                load(both, both, xr_sem.at[0, p - 1]).wait()
            with jax.named_scope(f"chan{p - 1}"):
                y = nn(mine, x_v[p - 1])
                for t in range(piece // LANES):
                    wide_v[pl.ds((p - 1) * (piece // LANES) + t, width, stride=steps), :] = y[:, t * LANES : (t + 1) * LANES]
    with jax.named_scope("hear1"):
        hear(1)
    a_v[...] = wide_v[...].astype(BF16)

    def spread(order, src_v, dst_v, send_sem, recv_sem):
        own = pl.ds(pl.multiple_of(row * tile, tile), tile)
        for dz, dx in order:
            d = lax.rem(z + dz, Z_SIDE) * X_SIDE + lax.rem(x + dx, X_SIDE)
            send(
                src_v.at[pl.ds(pl.multiple_of(d * tile, tile), tile)], dst_v.at[own], send_sem, recv_sem, (d, col)
            ).start()
        dst_v[own, :] = src_v[own, :]

    rest = pl.ds(0, (rows - 1) * tile)
    with jax.named_scope("spread1"):
        spread(FARTHEST_FIRST, a_v, ar_v, as_sem, ar_sem)

    per_group = GROUP // (2 * width)
    for g in range(cols // subs):
        wp = nn(back_v[...], wout_v[pl.ds(g * GROUP, GROUP), :])
        for i in range(per_group):
            wt_v[g * per_group + i] = jnp.transpose(wp[i * 2 * width : (i + 1) * 2 * width]).astype(BF16)

    with jax.named_scope("wait1"):
        load(ar_v.at[rest], ar_v.at[rest], ar_sem).wait()

    first = nn(outer_v[...], ar_v[...])
    high = rows * steps
    twist_cos, twist_sin = twist_v[:high], twist_v[high:]
    special = lax.min(j * rows + row, 1)
    for s in range(2):
        re = first[2 * s * high : (2 * s + 1) * high]
        im = first[(2 * s + 1) * high : (2 * s + 2) * high]
        turned = jnp.concatenate([re * twist_cos + im * twist_sin, im * twist_cos - re * twist_sin], axis=1).astype(BF16)
        u = nt(inner_v[0] if s == 0 else inner_v[special], turned)
        for t in range(2):
            wide_v[pl.ds(2 * t + s, LANES, stride=4), :] = u[:, t * LANES : (t + 1) * LANES]
    b_v[...] = wide_v[...].astype(BF16)

    with jax.named_scope("spread2"):
        spread(NEAREST_FIRST, b_v, br_v, bs_sem, br_sem.at[lax.div(z, 2)])
    chips = cols // 2
    half = chips // 2
    part = width // SETS
    lone = rows // SETS
    turn = lax.rem(z, 2)
    first_set = lax.div(z, 2)
    sets = [first_set] + [lax.rem(first_set + o, SETS) for o in (3 - 2 * turn, 1 + 2 * turn, 2)]

    def slot(who, q):
        of_set = pl.ds(pl.multiple_of(sets[q // HALVES] * part, part), part)
        return s_v.at[who, of_set, pl.ds(q % HALVES * (length // HALVES), length // HALVES)]

    def ring(d, t, q):
        who = lax.rem(col + (cols - 2 * (t - 1) if d == 0 else 2 * (t - 1)), cols)
        return send(slot(who, q), slot(who, q), gs_sem, gr_sem.at[d, t - 1, q], (row, right if d == 0 else left))

    def relay(d, t, q):
        who = lax.rem(col + (cols - 2 * t if d == 0 else 2 * t), cols)
        return send(slot(who, q), slot(who, q), cs_sem, cr_sem.at[t], (row, other))

    def uses(d, t):
        if t < half:
            return range(SETS * HALVES)
        return range(d, SETS * HALVES, 2)

    def share(q):
        for c in (ring(0, 1, q), ring(1, 1, q), relay(0, 0, q)):
            c.start()

    for q in range(SETS):
        with jax.named_scope(f"set{q}"):
            came = pl.ds(0, (lone if q else lone - 1) * tile)
            load(br_v.at[came], br_v.at[came], br_sem.at[sets[q]]).wait()
        base = pl.multiple_of(sets[q] * lone * tile, lone * tile)
        wide_v[pl.ds(base, lone * tile), :] = br_v[pl.ds(base, lone * tile), :].astype(F32)
        for k in range(steps):
            if k and k % (steps // HALVES) == 0:
                share(q * HALVES + k // (steps // HALVES) - 1)
            both = [wide_v[pl.ds(base + 2 * k + s, lone, stride=tile), :] for s in range(2)]
            s_v[col, pl.ds(pl.multiple_of(sets[q] * part, part), part), k * LANES : (k + 1) * LANES] = jnp.concatenate(
                both, 0
            ).astype(BF16)
        share(q * HALVES + HALVES - 1)

    def arrived(count, sem):
        blocks = s_v.at[pl.ds(0, count)]
        load(blocks, blocks, sem).wait()

    def add(which):
        acc_v[...] += nn(wt_v[which], s_v[pl.ds(2 * which, 2)].reshape(2 * width, length))

    def gather(t, step):
        if step == 0:
            with jax.named_scope(f"relayed{t}"):
                arrived(1 if t in (0, half) else 2, cr_sem.at[t])
            if t == 0:
                acc_v[...] = nn(wt_v[chip], s_v[pl.ds(2 * chip, 2)].reshape(2 * width, length))
        elif step == 1 and t:
            with jax.named_scope(f"add{t}"):
                add(lax.rem(chip + t, chips))
        elif step == 2 and 0 < t < half:
            with jax.named_scope(f"more{t}"):
                add(lax.rem(chip + chips - t, chips))

    for t in range(1, half + 1):
        for q in range(SETS * HALVES):
            for d in range(2):
                if q in uses(d, t):
                    with jax.named_scope(f"ring{t}q{q}d{d}"):
                        ring(d, t, q).wait_recv()
                    if t < half and q in uses(d, t + 1):
                        ring(d, t + 1, q).start()
                    relay(d, t, q).start()
            if q % 2 and q > 1:
                gather(t - 1, q // 2 - 1)
    for step in range(2):
        gather(half, step)
    with jax.named_scope("final"):
        for i in range(length // LANES):
            out_v[i * LANES : (i + 1) * LANES, :] = jnp.transpose(acc_v[:, i * LANES : (i + 1) * LANES]).astype(BF16)
    store = load(out_v, out, tab_sem.at[0])
    store.start()

    exchanged = x_v.at[pl.ds(0, 3 * PIECES * width // GROUP)]
    load(exchanged, exchanged, xs_sem).wait()
    arrived(cols // 2 - 1, gs_sem)
    arrived(cols // 2, cs_sem)
    load(a_v.at[rest], a_v.at[rest], as_sem).wait()
    load(b_v.at[rest], b_v.at[rest], bs_sem).wait()
    with jax.named_scope("stored"):
        store.wait()


def local(rows, cols, tokens, norm_gain, w_in, w_out):
    length, features = tokens.shape
    width, mapped = w_in.shape[1], w_out.shape[1]
    mix, back, outer, twist, inner, eye = tables(rows, width, length)
    high = rows * length // LANES
    half = cols // 4
    any_spec = pl.BlockSpec(memory_space=pl.ANY)
    dma = pltpu.SemaphoreType.DMA
    return pl.pallas_call(
        functools.partial(kernel, rows, cols),
        out_shape=jax.ShapeDtypeStruct((length, mapped), BF16),
        in_specs=[any_spec] * 10,
        out_specs=any_spec,
        scratch_shapes=[
            pltpu.VMEM((length, features), BF16),
            pltpu.VMEM((width, features), BF16),
            pltpu.VMEM((1, features), F32),
            pltpu.VMEM((width, features), BF16),
            pltpu.VMEM(w_out.shape, BF16),
            pltpu.VMEM(mix.shape, BF16),
            pltpu.VMEM(back.shape, BF16),
            pltpu.VMEM(outer.shape, BF16),
            pltpu.VMEM(twist.shape, F32),
            pltpu.VMEM(inner.shape, BF16),
            pltpu.VMEM(eye.shape, BF16),
            pltpu.VMEM((PIECES, GROUP, length // PIECES), BF16),
            pltpu.VMEM((2 * high, LANES), F32),
            pltpu.VMEM((2 * high, LANES), BF16),
            pltpu.VMEM((2 * high, LANES), BF16),
            pltpu.VMEM((2 * high, LANES), BF16),
            pltpu.VMEM((2 * high, LANES), BF16),
            pltpu.VMEM((cols, width, length), BF16),
            pltpu.VMEM((cols // 2, mapped, 2 * width), BF16),
            pltpu.VMEM((mapped, length), F32),
            pltpu.VMEM((length, mapped), BF16),
            dma((PIECES,)),
            dma((9,)),
            pltpu.SemaphoreType.REGULAR((2, 4)),
            dma,
            dma((2, PIECES)),
            dma,
            dma,
            dma,
            dma((SETS,)),
            dma,
            dma((2, half, SETS * HALVES)),
            dma,
            dma((half + 1,)),
        ],
        compiler_params=pltpu.CompilerParams(
            collective_id=0, has_side_effects=True, vmem_limit_bytes=60 * 1024 * 1024
        ),
    )(tokens, norm_gain.reshape(1, features), w_in.T, w_out, mix, back, outer, twist, inner, eye)


def solution(mesh):
    placed = (P("row", None), P(), P(None, "col"), P(None, "col"))
    return jax.shard_map(
        functools.partial(local, mesh.shape["row"], mesh.shape["col"]),
        mesh=mesh,
        in_specs=placed,
        out_specs=P("row", "col"),
        check_vma=False,
    )
```

time: 61.8 us -> 52.9 us (0.86)
  Pallas kernels: 58 us -> 51.1 us
  local copies, waits for them, and re-layouts: 3.62 us -> 1.67 us
    pallas_call x1, Pallas kernels: 58 us -> 51.1 us  [local(): pl.pallas_call(functools.partial(kernel, rows, cols), out_shape=jax.Shape...]
    unnamed x2 -> x1, local copies, waits for them, and re-layouts: 3.62 us -> 1.67 us
where the time goes in v2:
time: 52.9 us; the launch traced here: 52.7 us
  Pallas kernels  51.1 us (97%)
  local copies, waits for them, and re-layouts  1.67 us (3%)
    pallas_call x1, Pallas kernels, local(): pl.pallas_call(functools.partial(kernel, rows, cols), out_shape=jax.Shape...  51.1 us
    unnamed x1, local copies, waits for them, and re-layouts  1.67 us

profile of v2, /device:TPU:1, one launch (start us, length us, event | category | flops | bytes accessed | tf_op | source)
XLA Modules:
  0.0 52.7 jit_solution(7210899073802584952)
XLA Ops:
  0.0 51.1 %shard_map.100 = bf16[1024,128]{1,0:T(8,128)(2,1)} custom-call(bf16[1024,2048]{1,0:T(8,128)(2,1)} %tokens.1, f32[1,2048]{1,0:T(1,128)} %bitcast.3, bf16[64,2048]{1,0:T(8,128)(2,1)} %bitcast.2, bf16[1024,128]{1,0:T(8,128)(2,1)} %w_out.1, bf16[256,256]{1,0:T(8,128)(2,1)} %constant.12.clone.mix, bf16[256,256]{1,0:T(8,128)(2,1)} %constant.13.clone.back, ...), custom_call_target="tpu_custom_call" | custom-call | tf_op jit(solution)/shard_map/pallas_call | solution.py:341
  51.1 1.7 %copy.12 = bf16[1024,128]{1,0:T(8,128)(2,1)} copy(bf16[1024,128]{1,0:T(8,128)(2,1)} %shard_map.100) | data formatting | bytes 524288
